TPU v7x, 512 devices: a whole 4x8x8 slice. The times are simulated.
512 devices in a mesh: fs: 64 (over z, y), tp: 8 (over x, core).
Axes of the slice: x: 4, y: 8, z: 8, core: 2. Of those that a mesh axis runs over, the one named last changes fastest.
Arguments:
- tokens: bfloat16 [65536, 2048], P(('fs', 'tp')), may hold values from -8 to 8
- pre_mix_gain: float32 [2048], replicated, may hold values from 0.1 to 1.9
- post_mix_gain: float32 [2048], replicated, may hold values from 0.1 to 1.9
- pre_ffn_gain: float32 [2048], replicated, may hold values from 0.1 to 1.9
- post_ffn_gain: float32 [2048], replicated, may hold values from 0.1 to 1.9
- w_branch: bfloat16 [2048, 1024], P('fs', 'tp'), may hold values from -0.125 to 0.125
- w_gelu: bfloat16 [2048, 1024], P('fs', 'tp'), may hold values from -0.125 to 0.125
- conv_weight: bfloat16 [4, 1024], P(None, 'tp'), may hold values from -3 to 3
- w_rec: bfloat16 [2, 8, 128, 128], P(None, 'tp'), may hold values from -0.5 to 0.5
- w_inp: bfloat16 [2, 8, 128, 128], P(None, 'tp'), may hold values from -0.5 to 0.5
- decay: float32 [2, 1024], P(None, 'tp'), may hold values from 3 to 10
- out_weight_t: bfloat16 [2048, 1024], P('fs', 'tp'), may hold values from -0.1875 to 0.1875
- w_gate: bfloat16 [2048, 3072], P('fs', 'tp'), may hold values from -0.125 to 0.125
- w_up: bfloat16 [2048, 3072], P('fs', 'tp'), may hold values from -0.125 to 0.125
- down_weight_t: bfloat16 [2048, 3072], P('fs', 'tp'), may hold values from -0.109375 to 0.109375
Outputs:
- layer_out: bfloat16 [65536, 2048], P(('fs', 'tp'))
All inputs are finite; a program needn't handle non-finite values.
Results may differ from a plain program's by a relative error of at most 0.014.
Values may be sent and summed in bfloat16 or wider, within the bound.
A program may use at most 64 MiB of HBM per device.

v0:
```python
import jax
import jax.numpy as jnp
from jax import lax
from jax.sharding import PartitionSpec as P

EPS = 1e-06


def in_one_piece(arrays, axis, dim, along):
    both = jnp.concatenate(arrays, axis=along)
    whole, at, finished = (lax.all_gather(both, axis, axis=dim, tiled=True), 0, [])
    for a in arrays:
        finished.append(lax.slice_in_dim(whole, at, at + a.shape[along], axis=along))
        at += a.shape[along]
    return tuple(finished)


def normed(values, gain):
    factor = lax.rsqrt(jnp.mean(values * values, axis=-1, keepdims=True) + EPS)
    return values * factor * gain


def conv_short(branch, conv_weight):
    length = branch.shape[0]
    padded = jnp.pad(branch.astype(jnp.float32), ((2, 1), (0, 0)))
    weights = conv_weight.astype(jnp.float32)
    summed = weights[0] * padded[0:length]
    for offset in range(1, 4):
        summed = summed + weights[offset] * padded[offset : offset + length]
    return summed.astype(jnp.bfloat16)


def combine(earlier, later):
    return (earlier[0] * later[0], later[0] * earlier[1] + later[1])


def recurrence(conv_out, w_rec, w_inp, decay):
    length, channels = conv_out.shape
    blocks = w_rec.shape[0]
    grouped = conv_out.reshape(length, blocks, channels // blocks)
    rate_gate = jax.nn.sigmoid(
        jnp.einsum("lnc,ncd->lnd", grouped, w_rec, preferred_element_type=jnp.float32).reshape(
            length, channels
        )
    )
    inflow = jax.nn.sigmoid(
        jnp.einsum("lnc,ncd->lnd", grouped, w_inp, preferred_element_type=jnp.float32).reshape(
            length, channels
        )
    )
    log_retain = -8.0 * rate_gate * jax.nn.softplus(-decay)
    retain = jnp.exp(log_retain)
    feed = jnp.sqrt(-jnp.expm1(2.0 * log_retain)) * inflow * conv_out.astype(jnp.float32)
    unused_decay, states = lax.associative_scan(combine, (retain, feed), axis=0)
    return states


def gathered_product(normed_rows, left_weight, right_weight):
    row_piece = lax.all_gather(normed_rows, "tp", axis=0, tiled=True)
    return jnp.concatenate(
        [
            jnp.dot(row_piece, left_weight, preferred_element_type=jnp.float32),
            jnp.dot(row_piece, right_weight, preferred_element_type=jnp.float32),
        ],
        axis=1,
    )


def summed_rows(hidden, weight_t):
    return lax.psum_scatter(
        lax.dot_general(
            hidden, weight_t, (((1,), (1,)), ((), ())), preferred_element_type=jnp.float32
        ).astype(jnp.bfloat16),
        "tp",
        scatter_dimension=0,
        tiled=True,
    ).astype(jnp.float32)


def per_device(
    tokens,
    pre_mix_gain,
    post_mix_gain,
    pre_ffn_gain,
    post_ffn_gain,
    w_branch,
    w_gelu,
    conv_weight,
    w_rec,
    w_inp,
    decay,
    out_weight_t,
    w_gate,
    w_up,
    down_weight_t,
):
    branch_all, gelu_all, out_rows = in_one_piece((w_branch, w_gelu, out_weight_t), "fs", 0, 1)
    out_whole = lax.all_gather(out_rows, "tp", axis=1, tiled=True)
    stream = tokens.astype(jnp.float32)
    normed_in = normed(stream, pre_mix_gain).astype(jnp.bfloat16)
    both_in = gathered_product(normed_in, branch_all, gelu_all)
    channels = branch_all.shape[1]
    branch_in = both_in[:, :channels].astype(jnp.bfloat16)
    gelu_in = both_in[:, channels:].astype(jnp.bfloat16)
    conv_out = conv_short(branch_in, conv_weight)
    forward = recurrence(conv_out, w_rec[0], w_inp[0], decay[0])
    backward = jnp.flip(recurrence(jnp.flip(conv_out, 0), w_rec[1], w_inp[1], decay[1]), 0)
    mixer_hidden = (jax.nn.gelu(gelu_in.astype(jnp.float32)) * (forward + backward)).astype(
        jnp.bfloat16
    )
    own_hidden = lax.all_to_all(mixer_hidden, "tp", split_axis=0, concat_axis=1, tiled=True)
    mixer_sum = lax.dot_general(
        own_hidden, out_whole, (((1,), (1,)), ((), ())), preferred_element_type=jnp.float32
    )
    residual = (stream + normed(mixer_sum, post_mix_gain)).astype(jnp.bfloat16)
    middle = residual.astype(jnp.float32)
    normed_mid = normed(middle, pre_ffn_gain).astype(jnp.bfloat16)
    gate_all, up_all, down_all = in_one_piece((w_gate, w_up, down_weight_t), "fs", 0, 1)
    both_mid = gathered_product(normed_mid, gate_all, up_all)
    hidden_units = gate_all.shape[1]
    gate_proj = both_mid[:, :hidden_units]
    up_proj = both_mid[:, hidden_units:]
    ffn_hidden = (jax.nn.silu(gate_proj) * up_proj).astype(jnp.bfloat16)
    ffn_sum = summed_rows(ffn_hidden, down_all)
    return (middle + normed(ffn_sum, post_ffn_gain)).astype(jnp.bfloat16)


def solution(mesh):
    return jax.shard_map(
        per_device,
        mesh=mesh,
        in_specs=(
            P(("fs", "tp"), None),
            P(),
            P(),
            P(),
            P(),
            P("fs", "tp"),
            P("fs", "tp"),
            P(None, "tp"),
            P(None, "tp", None, None),
            P(None, "tp", None, None),
            P(None, "tp"),
            P("fs", "tp"),
            P("fs", "tp"),
            P("fs", "tp"),
            P("fs", "tp"),
        ),
        out_specs=P(("fs", "tp"), None),
        check_vma=False,
    )
```

profile of v0, /device:TPU:8, one launch (start us, length us, event | category | flops | bytes accessed | tf_op | source)
XLA Modules:
  0.0 372.8 jit_solution(1877080650165406262)
XLA Ops:
  6.5 1.3 pad_maximum_fusion.9
  7.9 1.2 fusion.29
  9.2 2.0 fusion.31
  11.3 85.9 %all-gather.8.cloned.1.call-done = bf16[2048,384]{1,0:T(8,128)(2,1)} async-done(((bf16[32,384]{1,0:T(8,128)(2,1)}), bf16[2048,384]{1,0:T(8,128)(2,1)}) %all-gather.8.cloned.1.call-update) | async-done | bytes 1572880 | tf_op jit(solution)/shard_map/all_gather | solution.py:11
  97.2 1.9 slice.729
  99.1 1.4 pad_maximum_fusion.4
  100.6 0.7 convert_element_type.60
  101.3 0.8 fusion.75
  102.1 32.2 %all-gather.6.cloned.1.call-done = bf16[1024,2048]{1,0:T(8,128)(2,1)} async-done(((bf16[128,2048]{1,0:T(8,128)(2,1)}), bf16[1024,2048]{1,0:T(8,128)(2,1)}) %all-gather.6.cloned.1.call-update) | async-done | bytes 4194320 | tf_op jit(solution)/shard_map/all_gather | solution.py:59
  134.3 3.5 fusion.25
  148.0 0.6 slice.596
  150.3 0.6 slice.551
  151.0 0.6 slice.600
  164.2 0.6 slice.641
  166.0 0.6 slice.635
  166.6 0.6 slice.676
  167.8 0.6 slice.629
  168.4 0.6 slice.678
  169.6 0.6 slice.623
  170.2 0.6 slice.680
  173.3 0.7 fusion.96
  174.1 0.8 fusion.92
  174.9 0.7 multiply_add_fusion.18
  175.6 0.6 pad_maximum_fusion.16
  176.3 0.7 multiply_add_fusion.14
  176.9 0.7 pad_maximum_fusion.14
  177.7 0.7 fusion.71
  178.4 0.7 pad_maximum_fusion.12
  179.2 0.7 fusion.69
  179.9 0.6 pad_maximum_fusion.10
  180.6 0.8 fusion.59
  181.4 0.6 pad_maximum_fusion.7
  182.1 0.7 pad_maximum_fusion.5
  182.9 0.6 pad_maximum_fusion.2
  183.6 1.7 pad.146
  185.4 1.7 pad.145
  187.1 0.8 fusion.94
  189.8 3.6 fusion.48
  193.6 10.2 %all_to_all.19 = bf16[8,128,128]{1,2,0:T(8,128)(2,1)S(1)} all-to-all(bf16[8,128,128]{1,2,0:T(8,128)(2,1)S(1)} %copy.16), channel_id=1, replica_groups=mesh['fs'=64,'tp'=8] {'tp'}, dimensions={0} | all-to-all | bytes 524288 | tf_op jit(solution)/shard_map/all_to_all | solution.py:111
  203.9 3.8 %multiply_reduce_fusion = (f32[128]{0:T(128)S(1)}, f32[128,2048]{1,0:T(8,128)S(1)}) fusion(bf16[128,1024]{0,1:T(8,128)(2,1)S(1)} %bitcast.42, bf16[2048,1024]{1,0:T(8,128)(2,1)} %all-gather.10.cloned.1.call-done), kind=kOutput, calls=%fused_computation.51 | convolution fusion | flops 537395072 | bytes 5505536 | tf_op jit(solution)/shard_map/dot_general | solution.py:112
  208.1 1.0 fusion.35
  209.3 58.9 %all-gather.14.cloned.1.call-done = bf16[2048,1152]{1,0:T(8,128)(2,1)} async-done(((bf16[32,1152]{1,0:T(8,128)(2,1)}), bf16[2048,1152]{1,0:T(8,128)(2,1)}) %all-gather.14.cloned.1.call-update) | async-done | bytes 4718608 | tf_op jit(solution)/shard_map/all_gather | solution.py:11
  268.2 36.3 %all-gather.12.cloned.1.call-done = bf16[1024,2048]{1,0:T(8,128)(2,1)} async-done(((bf16[128,2048]{1,0:T(8,128)(2,1)}), bf16[1024,2048]{1,0:T(8,128)(2,1)}) %all-gather.12.cloned.1.call-update) | async-done | bytes 4194320 | tf_op jit(solution)/shard_map/all_gather | solution.py:59
  304.5 5.0 %fusion.3 = f32[1024,384]{1,0:T(8,128)S(1)} fusion(bf16[1024,2048]{1,0:T(8,128)(2,1)} %all-gather.12.cloned.1.call-done, bf16[2048,1152]{1,0:T(8,128)(2,1)} %all-gather.14.cloned.1.call-done), kind=kOutput, calls=%fused_computation.4 | convolution fusion | flops 1610612736 | bytes 7340032 | tf_op jit(solution)/shard_map/dot_general | solution.py:62
  309.5 9.7 %convolution_convert_fusion = bf16[1024,2048]{1,0:T(8,128)(2,1)} fusion(bf16[2048,1152]{1,0:T(8,128)(2,1)} %all-gather.14.cloned.1.call-done, f32[1024,384]{1,0:T(8,128)S(1)} %fusion.3, bf16[1024,2048]{1,0:T(8,128)(2,1)} %all-gather.12.cloned.1.call-done), kind=kOutput, calls=%fused_computation | convolution fusion | flops 3225681920 | bytes 13107200 | tf_op jit(solution)/shard_map/dot_general | solution.py:71
  319.2 43.5 %reduce-scatter.2.cloned.1.call-done = bf16[128,2048]{1,0:T(8,128)(2,1)} async-done(((bf16[1024,2048]{1,0:T(8,128)(2,1)}), bf16[128,2048]{1,0:T(8,128)(2,1)}) %reduce-scatter.2.cloned.1.call-update) | async-done | bytes 524304 | tf_op jit(solution)/shard_map/reduce_scatter | solution.py:70
  362.6 1.2 fusion.27
  363.9 2.1 fusion.36
  (307 shorter events, 31.8 us)
Async XLA Ops:
  6.5 90.6 %all-gather.8.cloned.1.call-start = ((), (), s32[]{:S(2)}) async-start(), calls=%async_computation.3 | async-start | bytes 1597440 | tf_op jit(solution)/shard_map/all_gather | solution.py:11
  7.9 126.4 %all-gather.6.cloned.1.call-start = ((), (), s32[]{:S(2)}) async-start(), calls=%async_computation.2 | async-start | bytes 4718592 | tf_op jit(solution)/shard_map/all_gather | solution.py:59
  11.2 192.6 %all-gather.10.cloned.1.call-start = ((), (), s32[]{:S(2)}) async-start(), calls=%async_computation.4 | async-start | bytes 4718592 | tf_op jit(solution)/shard_map/all_gather | solution.py:98
  99.0 39.0 %copy-start.35 = (bf16[2,1,128,128]{3,2,1,0:T(8,128)(2,1)S(1)}, bf16[2,1,128,128]{3,2,1,0:T(8,128)(2,1)}, u32[]{:S(2)}) copy-start(bf16[2,1,128,128]{3,2,1,0:T(8,128)(2,1)} %param.23) | copy-start | bytes 196612
  99.1 169.1 %all-gather.14.cloned.1.call-start = ((), (), s32[]{:S(2)}) async-start(), calls=%async_computation.6 | async-start | bytes 4792320 | tf_op jit(solution)/shard_map/all_gather | solution.py:11
  100.6 203.9 %all-gather.12.cloned.1.call-start = ((), (), s32[]{:S(2)}) async-start(), calls=%async_computation.5 | async-start | bytes 4718592 | tf_op jit(solution)/shard_map/all_gather | solution.py:59
  102.1 36.4 %copy-start.36 = (bf16[2,1,128,128]{3,2,1,0:T(8,128)(2,1)S(1)}, bf16[2,1,128,128]{3,2,1,0:T(8,128)(2,1)}, u32[]{:S(2)}) copy-start(bf16[2,1,128,128]{3,2,1,0:T(8,128)(2,1)} %param.24) | copy-start | bytes 196612
  139.0 15.6 %copy-start.2 = (f32[1024,128]{1,0:T(8,128)}, f32[1024,128]{1,0:T(8,128)S(1)}, u32[]{:S(2)}) copy-start(f32[1024,128]{1,0:T(8,128)S(1)} %fusion.21) | copy-start | bytes 1572868
  141.6 11.7 %copy-start.15 = (f32[4,128]{1,0:T(4,128)}, f32[4,128]{1,0:T(4,128)S(1)}, u32[]{:S(2)}) copy-start(f32[4,128]{1,0:T(4,128)S(1)} %get-tuple-element.38) | copy-start | bytes 6148
  141.6 11.7 %copy-start.17 = (f32[4,128]{1,0:T(4,128)}, f32[4,128]{1,0:T(4,128)S(1)}, u32[]{:S(2)}) copy-start(f32[4,128]{1,0:T(4,128)S(1)} %get-tuple-element.37) | copy-start | bytes 6148
  155.8 17.5 %copy-start.1 = (f32[1024,128]{1,0:T(8,128)}, f32[1024,128]{1,0:T(8,128)S(1)}, u32[]{:S(2)}) copy-start(f32[1024,128]{1,0:T(8,128)S(1)} %fusion.24) | copy-start | bytes 1572868
  158.4 26.9 %copy-start.16 = (f32[4,128]{1,0:T(4,128)}, f32[4,128]{1,0:T(4,128)S(1)}, u32[]{:S(2)}) copy-start(f32[4,128]{1,0:T(4,128)S(1)} %get-tuple-element.42) | copy-start | bytes 6148
  158.4 26.9 %copy-start.18 = (f32[4,128]{1,0:T(4,128)}, f32[4,128]{1,0:T(4,128)S(1)}, u32[]{:S(2)}) copy-start(f32[4,128]{1,0:T(4,128)S(1)} %get-tuple-element.41) | copy-start | bytes 6148
  171.6 13.7 %slice-start.1 = ((f32[1024,128]{1,0:T(8,128)}), f32[1,128]{1,0:T(1,128)S(1)}, s32[]{:S(2)}) async-start(f32[1024,128]{1,0:T(8,128)} %copy-done.2), calls=%async_computation.9 | async-start | bytes 1024 | tf_op jit(solution)/shard_map/slice | solution.py:54
  174.0 13.1 %copy-start.24 = (f32[2,128]{1,0:T(2,128)S(1)}, f32[2,128]{1,0:T(2,128)}, u32[]{:S(2)}) copy-start(f32[2,128]{1,0:T(2,128)} %slice.661) | copy-start | bytes 3076
  174.0 13.1 %copy-start.25 = (f32[2,128]{1,0:T(2,128)S(1)}, f32[2,128]{1,0:T(2,128)}, u32[]{:S(2)}) copy-start(f32[2,128]{1,0:T(2,128)} %slice.662) | copy-start | bytes 3076
  174.0 13.1 %copy-start.26 = (f32[2,128]{1,0:T(2,128)S(1)}, f32[2,128]{1,0:T(2,128)}, u32[]{:S(2)}) copy-start(f32[2,128]{1,0:T(2,128)} %slice.660) | copy-start | bytes 3076
  174.0 13.1 %copy-start.27 = (f32[2,128]{1,0:T(2,128)S(1)}, f32[2,128]{1,0:T(2,128)}, u32[]{:S(2)}) copy-start(f32[2,128]{1,0:T(2,128)} %slice.664) | copy-start | bytes 3076
  175.6 12.4 %copy-start.22 = (f32[3,128]{1,0:T(4,128)S(1)}, f32[3,128]{1,0:T(4,128)}, u32[]{:S(2)}) copy-start(f32[3,128]{1,0:T(4,128)} %slice.653) | copy-start | bytes 4612
  175.6 12.4 %copy-start.23 = (f32[3,128]{1,0:T(4,128)S(1)}, f32[3,128]{1,0:T(4,128)}, u32[]{:S(2)}) copy-start(f32[3,128]{1,0:T(4,128)} %slice.670) | copy-start | bytes 4612
  176.2 11.8 %copy-start.34 = (f32[1,128]{1,0:T(1,128)S(1)}, f32[1,128]{1,0:T(1,128)}, u32[]{:S(2)}) copy-start(f32[1,128]{1,0:T(1,128)} %slice.651) | copy-start | bytes 1540
  176.2 11.8 %copy-start.13 = (f32[7,128]{1,0:T(8,128)S(1)}, f32[7,128]{1,0:T(8,128)}, u32[]{:S(2)}) copy-start(f32[7,128]{1,0:T(8,128)} %slice.647) | copy-start | bytes 10756
  176.2 11.8 %copy-start.14 = (f32[7,128]{1,0:T(8,128)S(1)}, f32[7,128]{1,0:T(8,128)}, u32[]{:S(2)}) copy-start(f32[7,128]{1,0:T(8,128)} %slice.672) | copy-start | bytes 10756
  177.6 10.4 %copy-start.33 = (f32[1,128]{1,0:T(1,128)S(1)}, f32[1,128]{1,0:T(1,128)}, u32[]{:S(2)}) copy-start(f32[1,128]{1,0:T(1,128)} %slice.716) | copy-start | bytes 1540
  177.6 10.5 %copy-start.11 = (f32[15,128]{1,0:T(8,128)S(1)}, f32[15,128]{1,0:T(8,128)}, u32[]{:S(2)}) copy-start(f32[15,128]{1,0:T(8,128)} %slice.641) | copy-start | bytes 23044
  177.7 10.5 %copy-start.12 = (f32[15,128]{1,0:T(8,128)S(1)}, f32[15,128]{1,0:T(8,128)}, u32[]{:S(2)}) copy-start(f32[15,128]{1,0:T(8,128)} %slice.674) | copy-start | bytes 23044
  178.4 9.8 %copy-start.32 = (f32[1,128]{1,0:T(1,128)S(1)}, f32[1,128]{1,0:T(1,128)}, u32[]{:S(2)}) copy-start(f32[1,128]{1,0:T(1,128)} %slice.715) | copy-start | bytes 1540
  179.1 9.1 %copy-start.9 = (f32[31,128]{1,0:T(8,128)S(1)}, f32[31,128]{1,0:T(8,128)}, u32[]{:S(2)}) copy-start(f32[31,128]{1,0:T(8,128)} %slice.635) | copy-start | bytes 47620
  179.1 9.1 %copy-start.10 = (f32[31,128]{1,0:T(8,128)S(1)}, f32[31,128]{1,0:T(8,128)}, u32[]{:S(2)}) copy-start(f32[31,128]{1,0:T(8,128)} %slice.676) | copy-start | bytes 47620
  179.9 8.4 %copy-start.31 = (f32[1,128]{1,0:T(1,128)S(1)}, f32[1,128]{1,0:T(1,128)}, u32[]{:S(2)}) copy-start(f32[1,128]{1,0:T(1,128)} %slice.714) | copy-start | bytes 1540
  180.5 7.8 %copy-start.7 = (f32[63,128]{1,0:T(8,128)S(1)}, f32[63,128]{1,0:T(8,128)}, u32[]{:S(2)}) copy-start(f32[63,128]{1,0:T(8,128)} %slice.629) | copy-start | bytes 96772
  180.5 7.8 %copy-start.8 = (f32[63,128]{1,0:T(8,128)S(1)}, f32[63,128]{1,0:T(8,128)}, u32[]{:S(2)}) copy-start(f32[63,128]{1,0:T(8,128)} %slice.678) | copy-start | bytes 96772
  181.4 7.0 %copy-start.30 = (f32[1,128]{1,0:T(1,128)S(1)}, f32[1,128]{1,0:T(1,128)}, u32[]{:S(2)}) copy-start(f32[1,128]{1,0:T(1,128)} %slice.713) | copy-start | bytes 1540
  182.1 6.4 %copy-start.5 = (f32[127,128]{1,0:T(8,128)S(1)}, f32[127,128]{1,0:T(8,128)}, u32[]{:S(2)}) copy-start(f32[127,128]{1,0:T(8,128)} %slice.623) | copy-start | bytes 195076
  182.1 6.4 %copy-start.6 = (f32[127,128]{1,0:T(8,128)S(1)}, f32[127,128]{1,0:T(8,128)}, u32[]{:S(2)}) copy-start(f32[127,128]{1,0:T(8,128)} %slice.680) | copy-start | bytes 195076
  182.1 6.4 %copy-start.29 = (f32[1,128]{1,0:T(1,128)S(1)}, f32[1,128]{1,0:T(1,128)}, u32[]{:S(2)}) copy-start(f32[1,128]{1,0:T(1,128)} %slice.712) | copy-start | bytes 1540
  182.9 5.8 %copy-start.28 = (f32[1,128]{1,0:T(1,128)S(1)}, f32[1,128]{1,0:T(1,128)}, u32[]{:S(2)}) copy-start(f32[1,128]{1,0:T(1,128)} %slice.711) | copy-start | bytes 1540
  185.4 3.6 slice-start
  188.6 1.0 copy-start.3
  188.6 1.2 copy-start.4
  193.4 14.3 %copy-start = (bf16[128,2048]{1,0:T(8,128)(2,1)S(1)}, bf16[128,2048]{1,0:T(8,128)(2,1)}, u32[]{:S(2)}) copy-start(bf16[128,2048]{1,0:T(8,128)(2,1)} %param.15) | copy-start | bytes 1572868
  193.4 14.2 %copy-start.19 = (f32[2048]{0:T(1024)S(1)}, f32[2048]{0:T(1024)}, u32[]{:S(2)}) copy-start(f32[2048]{0:T(1024)} %param.17) | copy-start | bytes 24580
  193.6 14.5 %copy-start.20 = (f32[2048]{0:T(1024)S(1)}, f32[2048]{0:T(1024)}, u32[]{:S(2)}) copy-start(f32[2048]{0:T(1024)} %param.18) | copy-start | bytes 24580
  209.1 153.6 %reduce-scatter.2.cloned.1.call-start = ((), (), s32[]{:S(2)}) async-start(), calls=%async_computation.7 | async-start | bytes 4718592 | tf_op jit(solution)/shard_map/reduce_scatter | solution.py:70
  319.2 44.7 %copy-start.21 = (f32[2048]{0:T(1024)S(1)}, f32[2048]{0:T(1024)}, u32[]{:S(2)}) copy-start(f32[2048]{0:T(1024)} %param.19) | copy-start | bytes 24580
Sparse Core Ops, SparseCore 0:
  10.3 86.7 all-gather.7
  99.3 34.8 all-gather.5
  136.4 40.8 all-gather.9
  180.1 87.9 all-gather.13
  270.2 34.2 all-gather.11
  319.3 43.2 reduce-scatter.1
where the time goes:
time: 374 us; the launch traced here: 373 us
  waiting for transfers between devices  257 us (69%)
  local copies, waits for them, and re-layouts  39.3 us (11%)
  matrix products  27.3 us (7%)
  other arithmetic  23.8 us (6%)
  between operations  15 us (4%)
  blocking collectives  10.2 us (3%)
    all_gather x2, waiting for transfers between devices, in_one_piece(): lax.all_gather(both, axis, axis=dim, tiled=True)  145 us
    all_gather x2, waiting for transfers between devices, gathered_product(): row_piece = lax.all_gather(normed_rows, 'tp', axis=0, tiled=True)  68.5 us
    reduce_scatter x1, waiting for transfers between devices, summed_rows(): lax.psum_scatter(lax.dot_general(hidden, weight_t, (((1,), (1,)), ((), ()...  43.5 us
    slice x122, local copies, waits for them, and re-layouts, recurrence(): unused_decay, states = lax.associative_scan(combine, (retain, feed), axis=0)  32.3 us
    all_to_all x1, blocking collectives, per_device(): lax.all_to_all(mixer_hidden, 'tp', split_axis=0, concat_axis=1, tiled=True)  10.2 us
    dot_general x1, matrix products, summed_rows(): lax.dot_general(hidden, weight_t, (((1,), (1,)), ((), ())), preferred_ele...  9.7 us
    dot_general x2, matrix products, gathered_product(): jnp.dot(row_piece, left_weight, preferred_element_type=jnp.float32)  8.54 us
  transfers between devices with their start and end apart: 6, of which 5 were waited for; matrix products, arithmetic and copies ran while one was open for 19% of the time, Pallas kernels for 0%

commit v1 on v0

--- a/solution.py
+++ b/solution.py
@@ -2,6 +2,7 @@
 import jax.numpy as jnp
 from jax import lax
 from jax.sharding import PartitionSpec as P
+from jax.lax import axis_index, axis_size, ppermute
 
 EPS = 1e-06
 
@@ -56,7 +57,26 @@
 
 
 def gathered_product(normed_rows, left_weight, right_weight):
-    row_piece = lax.all_gather(normed_rows, "tp", axis=0, tiled=True)
+    opened = axis_size("tp")
+    r2, p_next, f_now = (opened, axis_index("tp"), normed_rows.shape[0])
+    frames = [(b, (b + 1) % r2) for b in range(r2)]
+    row_piece = jnp.zeros(
+        (*normed_rows.shape[:0], r2 * f_now, *normed_rows.shape[1:]), normed_rows.dtype
+    )
+    row_piece = lax.dynamic_update_slice_in_dim(row_piece, normed_rows, p_next * f_now, axis=0)
+    runs = [(b, (b - 1) % r2) for b in range(r2)]
+    block_last = local_now = normed_rows
+    before = r2 // 2
+    for ix in tuple(range(1, before + 1)):
+        block_last = ppermute(block_last, "tp", perm=frames)
+        row_piece = lax.dynamic_update_slice_in_dim(
+            row_piece, block_last, (p_next - ix) % r2 * f_now, axis=0
+        )
+        if ix < r2 - before:
+            local_now = ppermute(local_now, axis_name="tp", perm=runs)
+            row_piece = lax.dynamic_update_slice_in_dim(
+                row_piece, local_now, (p_next + ix) % r2 * f_now, axis=0
+            )
     return jnp.concatenate(
         [
             jnp.dot(row_piece, left_weight, preferred_element_type=jnp.float32),

time: 374 us -> 353 us (0.944)
  waiting for transfers between devices: 257 us -> 189 us
  local copies, waits for them, and re-layouts: 39.3 us -> 60.2 us
  starting transfers between devices: 0.39 us -> 18.5 us
  other arithmetic: 23.8 us -> 30.1 us
    all_gather x2 -> x0, waiting for transfers between devices: 68.5 us -> none  [gathered_product(): row_piece = lax.all_gather(normed_rows, 'tp', axis=0, tiled=True)]
    ppermute x0 -> x14, waiting for transfers between devices: none -> 60.7 us  [the longest x8 60.5 us: gathered_product(): block_last = ppermute(block_last, 'tp', perm=frames)]
    all_gather x2, waiting for transfers between devices: 145 us -> 89.2 us  [in_one_piece(): lax.all_gather(both, axis, axis=dim, tiled=True)]
    ppermute x0 -> x14, starting transfers between devices: none -> 18.3 us  [the longest x6 18.3 us: gathered_product(): local_now = ppermute(local_now, axis_name='tp', perm=runs)]
    dynamic_update_slice x0 -> x14, local copies, waits for them, and re-layouts: none -> 11.9 us  [the longest x8 6.81 us: gathered_product(): lax.dynamic_update_slice_in_dim(row_piece, block_last, (p_next - ix) % r2...]
    dot_general x1 -> x2, matrix products: 3.57 us -> 8.8 us  [gathered_product(): jnp.dot(row_piece, right_weight, preferred_element_type=jnp.float32)]
    another operation x0 -> x2, local copies, waits for them, and re-layouts: none -> 5.03 us
    dot_general x2 -> x1, matrix products: 8.54 us -> 3.57 us  [gathered_product(): jnp.dot(row_piece, left_weight, preferred_element_type=jnp.float32)]
  transfers between devices with their start and end apart: 6 -> 18, of which waited for: 5 -> 11; matrix products, arithmetic and copies ran while one was open for 19% -> 28% of each run, Pallas kernels for 0% -> 0%
where the time goes in v1:
time: 353 us; the launch traced here: 352 us
  waiting for transfers between devices  189 us (54%)
  local copies, waits for them, and re-layouts  60.2 us (17%)
  other arithmetic  30.1 us (9%)
  matrix products  29.1 us (8%)
  starting transfers between devices  18.5 us (5%)
  between operations  14.4 us (4%)
  blocking collectives  9.92 us (3%)
    all_gather x2, waiting for transfers between devices, in_one_piece(): lax.all_gather(both, axis, axis=dim, tiled=True)  89.2 us
    ppermute x8, waiting for transfers between devices, gathered_product(): block_last = ppermute(block_last, 'tp', perm=frames)  60.5 us
    reduce_scatter x1, waiting for transfers between devices, summed_rows(): lax.psum_scatter(lax.dot_general(hidden, weight_t, (((1,), (1,)), ((), ()...  39.3 us
    slice x122, local copies, waits for them, and re-layouts, recurrence(): unused_decay, states = lax.associative_scan(combine, (retain, feed), axis=0)  36.4 us
    ppermute x6, starting transfers between devices, gathered_product(): local_now = ppermute(local_now, axis_name='tp', perm=runs)  18.3 us
    all_to_all x1, blocking collectives, per_device(): lax.all_to_all(mixer_hidden, 'tp', split_axis=0, concat_axis=1, tiled=True)  9.92 us
    dot_general x1, matrix products, summed_rows(): lax.dot_general(hidden, weight_t, (((1,), (1,)), ((), ())), preferred_ele...  9.72 us
    dot_general x2, matrix products, gathered_product(): jnp.dot(row_piece, right_weight, preferred_element_type=jnp.float32)  8.8 us
  transfers between devices with their start and end apart: 18, of which 11 were waited for; matrix products, arithmetic and copies ran while one was open for 28% of the time, Pallas kernels for 0%

profile of v1, /device:TPU:8, one launch (start us, length us, event | category | flops | bytes accessed | tf_op | source)
XLA Modules:
  0.0 351.5 jit_solution(8098987015684253964)
XLA Ops:
  6.6 1.4 pad_maximum_fusion.9
  8.1 89.2 %all-gather.4.cloned.1.call-done = bf16[2048,384]{1,0:T(8,128)(2,1)} async-done(((bf16[32,384]{1,0:T(8,128)(2,1)}), bf16[2048,384]{1,0:T(8,128)(2,1)}) %all-gather.4.cloned.1.call-update) | async-done | bytes 1572880 | tf_op jit(solution)/shard_map/all_gather | solution.py:12
  97.2 1.9 slice.729
  99.2 1.2 fusion.27
  100.4 2.5 broadcast.164.clone
  102.9 1.0 constant_dynamic-update-slice_fusion.15
  103.9 3.0 collective-permute-start.1
  106.9 6.9 %collective-permute-done = bf16[128,2048]{1,0:T(8,128)(2,1)S(1)} collective-permute-done((bf16[128,2048]{1,0:T(8,128)(2,1)S(1)}, bf16[128,2048]{1,0:T(8,128)(2,1)S(1)}, u32[]{:S(2)}, u32[]{:S(2)}) %collective-permute-start) | collective-permute-done | bytes 524320 | tf_op jit(solution)/shard_map/ppermute | solution.py:71
  114.7 3.5 %collective-permute-start.3 = (bf16[128,2048]{1,0:T(8,128)(2,1)S(1)}, bf16[128,2048]{1,0:T(8,128)(2,1)S(1)}, u32[]{:S(2)}, u32[]{:S(2)}) collective-permute-start(bf16[128,2048]{1,0:T(8,128)(2,1)S(1)} %collective-permute-done.1), channel_id=1, source_target_pairs={{0,7},{1,0},{2,1},{3,2},{4,3},{5,4},{6,5},{7,6},{8,15},{9,8},{10,9... | collective-permute-start | bytes 1572872 | tf_op jit(solution)/shard_map/ppermute | solution.py:76
  118.7 11.7 %collective-permute-done.2 = bf16[128,2048]{1,0:T(8,128)(2,1)S(1)} collective-permute-done((bf16[128,2048]{1,0:T(8,128)(2,1)S(1)}, bf16[128,2048]{1,0:T(8,128)(2,1)S(1)}, u32[]{:S(2)}, u32[]{:S(2)}) %collective-permute-start.2) | collective-permute-done | bytes 524320 | tf_op jit(solution)/shard_map/ppermute | solution.py:71
  131.3 0.9 constant_dynamic-update-slice_fusion.13
  132.1 2.9 collective-permute-start.5
  135.9 9.4 %collective-permute-done.4 = bf16[128,2048]{1,0:T(8,128)(2,1)S(1)} collective-permute-done((bf16[128,2048]{1,0:T(8,128)(2,1)S(1)}, bf16[128,2048]{1,0:T(8,128)(2,1)S(1)}, u32[]{:S(2)}, u32[]{:S(2)}) %collective-permute-start.4) | collective-permute-done | bytes 524320 | tf_op jit(solution)/shard_map/ppermute | solution.py:71
  145.4 0.9 constant_dynamic-update-slice_fusion.11
  147.9 7.3 %collective-permute-done.6 = bf16[128,2048]{1,0:T(8,128)(2,1)S(1)} collective-permute-done((bf16[128,2048]{1,0:T(8,128)(2,1)S(1)}, bf16[128,2048]{1,0:T(8,128)(2,1)S(1)}, u32[]{:S(2)}, u32[]{:S(2)}) %collective-permute-start.6) | collective-permute-done | bytes 524320 | tf_op jit(solution)/shard_map/ppermute | solution.py:71
  156.0 3.6 %fusion.23 = f32[1024,128]{1,0:T(8,128)S(1)} fusion(bf16[1024,2048]{1,0:T(8,128)(2,1)} %constant_dynamic-update-slice_fusion.8, bf16[2048,384]{1,0:T(8,128)(2,1)} %all-gather.4.cloned.1.call-done), kind=kOutput, calls=%fused_computation.38 | convolution fusion | flops 537133056 | bytes 5242880 | tf_op jit(solution)/shard_map/dot_general | solution.py:82
  176.0 0.9 slice.604
  178.5 1.1 fusion.101
  179.6 1.3 fusion.22
  182.2 1.4 slice.616
  183.5 1.0 fusion.81
  198.5 0.9 slice.617
  199.4 0.9 slice.682
  210.3 0.9 fusion.57
  212.0 1.0 fusion.55
  213.7 1.7 pad.146
  215.4 1.7 pad.145
  223.1 0.9 fusion.56
  225.7 3.8 %fusion.48 = bf16[1024,128]{1,0:T(8,128)(2,1)S(1)} fusion(bf16[1024,2048]{1,0:T(8,128)(2,1)} %constant_dynamic-update-slice_fusion.8, bf16[2048,384]{1,0:T(8,128)(2,1)} %all-gather.4.cloned.1.call-done, f32[1024,128]{1,0:T(8,128)S(1)} %rev.9, f32[1024,128]{1,0:T(8,128)} %pad.145, f32[1024,128]{1,0:T(8,128)S(1)} %copy-done.5), kind=kOutput, calls=%fused_computation.62 | convolution fusion | flops 538705920 | bytes 6553600 | tf_op jit(solution)/shard_map/dot_general | solution.py:83
  229.8 9.9 %all_to_all.19 = bf16[8,128,128]{1,2,0:T(8,128)(2,1)S(1)} all-to-all(bf16[8,128,128]{1,2,0:T(8,128)(2,1)S(1)} %copy.16), channel_id=1, replica_groups=mesh['fs'=64,'tp'=8] {'tp'}, dimensions={0} | all-to-all | bytes 524288 | tf_op jit(solution)/shard_map/all_to_all | solution.py:131
  239.7 3.8 %multiply_reduce_fusion = (f32[128]{0:T(128)S(1)}, f32[128,2048]{1,0:T(8,128)S(1)}) fusion(bf16[128,1024]{0,1:T(8,128)(2,1)S(1)} %bitcast.42, bf16[2048,1024]{1,0:T(8,128)(2,1)} %all-gather.6.cloned.1.call-done), kind=kOutput, calls=%fused_computation.51 | convolution fusion | flops 537395072 | bytes 5505536 | tf_op jit(solution)/shard_map/dot_general | solution.py:132
  243.9 2.6 broadcast.164
  246.4 1.0 constant_dynamic-update-slice_fusion.7
  247.4 3.0 collective-permute-start.8
  250.4 6.9 %collective-permute-done.7 = bf16[128,2048]{1,0:T(8,128)(2,1)S(1)} collective-permute-done((bf16[128,2048]{1,0:T(8,128)(2,1)S(1)}, bf16[128,2048]{1,0:T(8,128)(2,1)S(1)}, u32[]{:S(2)}, u32[]{:S(2)}) %collective-permute-start.7) | collective-permute-done | bytes 524320 | tf_op jit(solution)/shard_map/ppermute | solution.py:71
  257.2 3.0 collective-permute-start.10
  260.2 6.9 %collective-permute-done.9 = bf16[128,2048]{1,0:T(8,128)(2,1)S(1)} collective-permute-done((bf16[128,2048]{1,0:T(8,128)(2,1)S(1)}, bf16[128,2048]{1,0:T(8,128)(2,1)S(1)}, u32[]{:S(2)}, u32[]{:S(2)}) %collective-permute-start.9) | collective-permute-done | bytes 524320 | tf_op jit(solution)/shard_map/ppermute | solution.py:71
  268.7 3.0 collective-permute-start.12
  271.7 0.9 constant_dynamic-update-slice_fusion.4
  272.6 4.3 %collective-permute-done.11 = bf16[128,2048]{1,0:T(8,128)(2,1)S(1)} collective-permute-done((bf16[128,2048]{1,0:T(8,128)(2,1)S(1)}, bf16[128,2048]{1,0:T(8,128)(2,1)S(1)}, u32[]{:S(2)}, u32[]{:S(2)}) %collective-permute-start.11) | collective-permute-done | bytes 524320 | tf_op jit(solution)/shard_map/ppermute | solution.py:71
  277.7 0.9 constant_dynamic-update-slice_fusion.2
  279.5 7.2 %collective-permute-done.13 = bf16[128,2048]{1,0:T(8,128)(2,1)S(1)} collective-permute-done((bf16[128,2048]{1,0:T(8,128)(2,1)S(1)}, bf16[128,2048]{1,0:T(8,128)(2,1)S(1)}, u32[]{:S(2)}, u32[]{:S(2)}) %collective-permute-start.13) | collective-permute-done | bytes 524320 | tf_op jit(solution)/shard_map/ppermute | solution.py:71
  286.7 0.9 constant_dynamic-update-slice_fusion
  287.6 5.0 %fusion.1 = f32[1024,384]{1,0:T(8,128)S(1)} fusion(bf16[1024,2048]{1,0:T(8,128)(2,1)} %constant_dynamic-update-slice_fusion, bf16[2048,1152]{1,0:T(8,128)(2,1)} %all-gather.8.cloned.1.call-done), kind=kOutput, calls=%fused_computation.2 | convolution fusion | flops 1610612736 | bytes 7340032 | tf_op jit(solution)/shard_map/dot_general | solution.py:83
  292.5 9.7 %convolution_convert_fusion = bf16[1024,2048]{1,0:T(8,128)(2,1)} fusion(bf16[2048,1152]{1,0:T(8,128)(2,1)} %all-gather.8.cloned.1.call-done, f32[1024,384]{1,0:T(8,128)S(1)} %fusion.1, bf16[1024,2048]{1,0:T(8,128)(2,1)} %constant_dynamic-update-slice_fusion), kind=kOutput, calls=%fused_computation | convolution fusion | flops 3225681920 | bytes 13107200 | tf_op jit(solution)/shard_map/dot_general | solution.py:91
  302.3 39.3 %reduce-scatter.2.cloned.1.call-done = bf16[128,2048]{1,0:T(8,128)(2,1)} async-done(((bf16[1024,2048]{1,0:T(8,128)(2,1)}), bf16[128,2048]{1,0:T(8,128)(2,1)}) %reduce-scatter.2.cloned.1.call-update) | async-done | bytes 524304 | tf_op jit(solution)/shard_map/reduce_scatter | solution.py:90
  341.6 1.2 fusion.25
  342.9 2.1 fusion.34
  (339 shorter events, 61.3 us)
Async XLA Ops:
  6.5 96.4 %copy-start = (bf16[128,2048]{1,0:T(8,128)(2,1)S(1)}, bf16[128,2048]{1,0:T(8,128)(2,1)}, u32[]{:S(2)}) copy-start(bf16[128,2048]{1,0:T(8,128)(2,1)} %param.15) | copy-start | bytes 1572868
  6.5 96.4 %copy-start.19 = (f32[2048]{0:T(1024)S(1)}, f32[2048]{0:T(1024)}, u32[]{:S(2)}) copy-start(f32[2048]{0:T(1024)} %param.16) | copy-start | bytes 24580
  6.5 107.2 %copy-start.12 = (bf16[32,384]{1,0:T(8,128)(2,1)S(1)}, bf16[32,384]{1,0:T(8,128)(2,1)}, u32[]{:S(2)}) copy-start(bf16[32,384]{1,0:T(8,128)(2,1)} %param.27) | copy-start | bytes 73732
  6.5 107.2 %copy-start.11 = (bf16[32,384]{1,0:T(8,128)(2,1)S(1)}, bf16[32,384]{1,0:T(8,128)(2,1)}, u32[]{:S(2)}) copy-start(bf16[32,384]{1,0:T(8,128)(2,1)} %param.28) | copy-start | bytes 73732
  6.5 107.2 %copy-start.10 = (bf16[32,384]{1,0:T(8,128)(2,1)S(1)}, bf16[32,384]{1,0:T(8,128)(2,1)}, u32[]{:S(2)}) copy-start(bf16[32,384]{1,0:T(8,128)(2,1)} %param.29) | copy-start | bytes 73732
  6.5 107.9 %copy-start.29 = (bf16[4,128]{1,0:T(4,128)(2,1)S(1)}, bf16[4,128]{1,0:T(4,128)(2,1)}, u32[]{:S(2)}) copy-start(bf16[4,128]{1,0:T(4,128)(2,1)} %param.22) | copy-start | bytes 3076
  6.6 111.7 %copy-start.30 = (f32[2,128]{1,0:T(2,128)S(1)}, f32[2,128]{1,0:T(2,128)}, u32[]{:S(2)}) copy-start(f32[2,128]{1,0:T(2,128)} %param.25) | copy-start | bytes 3076
  6.6 90.7 %all-gather.4.cloned.1.call-start = ((), (), s32[]{:S(2)}) async-start(), calls=%async_computation.2 | async-start | bytes 1597440 | tf_op jit(solution)/shard_map/all_gather | solution.py:12
  8.0 231.7 %all-gather.6.cloned.1.call-start = ((), (), s32[]{:S(2)}) async-start(), calls=%async_computation.3 | async-start | bytes 4718592 | tf_op jit(solution)/shard_map/all_gather | solution.py:118
  99.1 188.4 %all-gather.8.cloned.1.call-start = ((), (), s32[]{:S(2)}) async-start(), calls=%async_computation.4 | async-start | bytes 4792320 | tf_op jit(solution)/shard_map/all_gather | solution.py:12
  103.9 9.8 %collective-permute-start = (bf16[128,2048]{1,0:T(8,128)(2,1)S(1)}, bf16[128,2048]{1,0:T(8,128)(2,1)S(1)}, u32[]{:S(2)}, u32[]{:S(2)}) collective-permute-start(bf16[128,2048]{1,0:T(8,128)(2,1)S(1)} %get-tuple-element.10), channel_id=1, source_target_pairs={{0,1},{1,2},{2,3},{3,4},{4,5},{5,6},{6,7},{7,0},{8,9},{9,10},{10,1... | collective-permute-start | bytes 1572872 | tf_op jit(solution)/shard_map/ppermute | solution.py:71
  103.9 10.8 %collective-permute-start.1 = (bf16[128,2048]{1,0:T(8,128)(2,1)S(1)}, bf16[128,2048]{1,0:T(8,128)(2,1)S(1)}, u32[]{:S(2)}, u32[]{:S(2)}) collective-permute-start(bf16[128,2048]{1,0:T(8,128)(2,1)S(1)} %get-tuple-element.10), channel_id=1, source_target_pairs={{0,7},{1,0},{2,1},{3,2},{4,3},{5,4},{6,5},{7,6},{8,15},{9,8},{10,9... | collective-permute-start | bytes 1572872 | tf_op jit(solution)/shard_map/ppermute | solution.py:76
  113.7 16.7 %collective-permute-start.2 = (bf16[128,2048]{1,0:T(8,128)(2,1)S(1)}, bf16[128,2048]{1,0:T(8,128)(2,1)S(1)}, u32[]{:S(2)}, u32[]{:S(2)}) collective-permute-start(bf16[128,2048]{1,0:T(8,128)(2,1)S(1)} %collective-permute-done), channel_id=1, source_target_pairs={{0,1},{1,2},{2,3},{3,4},{4,5},{5,6},{6,7},{7,0},{8,9},{9,10},{10,1... | collective-permute-start | bytes 1572872 | tf_op jit(solution)/shard_map/ppermute | solution.py:71
  114.4 227.2 %reduce-scatter.2.cloned.1.call-start = ((), (), s32[]{:S(2)}) async-start(), calls=%async_computation.5 | async-start | bytes 4718592 | tf_op jit(solution)/shard_map/reduce_scatter | solution.py:90
  114.7 17.4 %collective-permute-start.3 = (bf16[128,2048]{1,0:T(8,128)(2,1)S(1)}, bf16[128,2048]{1,0:T(8,128)(2,1)S(1)}, u32[]{:S(2)}, u32[]{:S(2)}) collective-permute-start(bf16[128,2048]{1,0:T(8,128)(2,1)S(1)} %collective-permute-done.1), channel_id=1, source_target_pairs={{0,7},{1,0},{2,1},{3,2},{4,3},{5,4},{6,5},{7,6},{8,15},{9,8},{10,9... | collective-permute-start | bytes 1572872 | tf_op jit(solution)/shard_map/ppermute | solution.py:76
  130.4 14.9 %collective-permute-start.4 = (bf16[128,2048]{1,0:T(8,128)(2,1)S(1)}, bf16[128,2048]{1,0:T(8,128)(2,1)S(1)}, u32[]{:S(2)}, u32[]{:S(2)}) collective-permute-start(bf16[128,2048]{1,0:T(8,128)(2,1)S(1)} %collective-permute-done.2), channel_id=1, source_target_pairs={{0,1},{1,2},{2,3},{3,4},{4,5},{5,6},{6,7},{7,0},{8,9},{9,10},{10,1... | collective-permute-start | bytes 1572872 | tf_op jit(solution)/shard_map/ppermute | solution.py:71
  132.1 14.9 %collective-permute-start.5 = (bf16[128,2048]{1,0:T(8,128)(2,1)S(1)}, bf16[128,2048]{1,0:T(8,128)(2,1)S(1)}, u32[]{:S(2)}, u32[]{:S(2)}) collective-permute-start(bf16[128,2048]{1,0:T(8,128)(2,1)S(1)} %collective-permute-done.3), channel_id=1, source_target_pairs={{0,7},{1,0},{2,1},{3,2},{4,3},{5,4},{6,5},{7,6},{8,15},{9,8},{10,9... | collective-permute-start | bytes 1572872 | tf_op jit(solution)/shard_map/ppermute | solution.py:76
  145.3 9.8 %collective-permute-start.6 = (bf16[128,2048]{1,0:T(8,128)(2,1)S(1)}, bf16[128,2048]{1,0:T(8,128)(2,1)S(1)}, u32[]{:S(2)}, u32[]{:S(2)}) collective-permute-start(bf16[128,2048]{1,0:T(8,128)(2,1)S(1)} %collective-permute-done.4), channel_id=1, source_target_pairs={{0,1},{1,2},{2,3},{3,4},{4,5},{5,6},{6,7},{7,0},{8,9},{9,10},{10,1... | collective-permute-start | bytes 1572872 | tf_op jit(solution)/shard_map/ppermute | solution.py:71
  160.7 17.5 %copy-start.2 = (f32[1024,128]{1,0:T(8,128)}, f32[1024,128]{1,0:T(8,128)S(1)}, u32[]{:S(2)}) copy-start(f32[1024,128]{1,0:T(8,128)S(1)} %fusion.19) | copy-start | bytes 1572868
  163.4 13.6 %copy-start.15 = (f32[4,128]{1,0:T(4,128)}, f32[4,128]{1,0:T(4,128)S(1)}, u32[]{:S(2)}) copy-start(f32[4,128]{1,0:T(4,128)S(1)} %get-tuple-element.42) | copy-start | bytes 6148
  163.4 13.6 %copy-start.17 = (f32[4,128]{1,0:T(4,128)}, f32[4,128]{1,0:T(4,128)S(1)}, u32[]{:S(2)}) copy-start(f32[4,128]{1,0:T(4,128)S(1)} %get-tuple-element.41) | copy-start | bytes 6148
  180.9 20.7 %copy-start.1 = (f32[1024,128]{1,0:T(8,128)}, f32[1024,128]{1,0:T(8,128)S(1)}, u32[]{:S(2)}) copy-start(f32[1024,128]{1,0:T(8,128)S(1)} %fusion.22) | copy-start | bytes 1572868
  185.4 29.9 %copy-start.16 = (f32[4,128]{1,0:T(4,128)}, f32[4,128]{1,0:T(4,128)S(1)}, u32[]{:S(2)}) copy-start(f32[4,128]{1,0:T(4,128)S(1)} %get-tuple-element.46) | copy-start | bytes 6148
  185.4 29.9 %copy-start.18 = (f32[4,128]{1,0:T(4,128)}, f32[4,128]{1,0:T(4,128)S(1)}, u32[]{:S(2)}) copy-start(f32[4,128]{1,0:T(4,128)S(1)} %get-tuple-element.45) | copy-start | bytes 6148
  199.4 16.0 %slice-start.1 = ((f32[1024,128]{1,0:T(8,128)}), f32[1,128]{1,0:T(1,128)S(1)}, s32[]{:S(2)}) async-start(f32[1024,128]{1,0:T(8,128)} %copy-done.2), calls=%async_computation.7 | async-start | bytes 1024 | tf_op jit(solution)/shard_map/slice | solution.py:55
  202.3 14.8 %copy-start.25 = (f32[2,128]{1,0:T(2,128)S(1)}, f32[2,128]{1,0:T(2,128)}, u32[]{:S(2)}) copy-start(f32[2,128]{1,0:T(2,128)} %slice.661) | copy-start | bytes 3076
  202.3 14.8 %copy-start.26 = (f32[2,128]{1,0:T(2,128)S(1)}, f32[2,128]{1,0:T(2,128)}, u32[]{:S(2)}) copy-start(f32[2,128]{1,0:T(2,128)} %slice.662) | copy-start | bytes 3076
  202.3 14.8 %copy-start.27 = (f32[2,128]{1,0:T(2,128)S(1)}, f32[2,128]{1,0:T(2,128)}, u32[]{:S(2)}) copy-start(f32[2,128]{1,0:T(2,128)} %slice.660) | copy-start | bytes 3076
  202.3 14.8 %copy-start.28 = (f32[2,128]{1,0:T(2,128)S(1)}, f32[2,128]{1,0:T(2,128)}, u32[]{:S(2)}) copy-start(f32[2,128]{1,0:T(2,128)} %slice.664) | copy-start | bytes 3076
  203.9 14.1 %copy-start.23 = (f32[3,128]{1,0:T(4,128)S(1)}, f32[3,128]{1,0:T(4,128)}, u32[]{:S(2)}) copy-start(f32[3,128]{1,0:T(4,128)} %slice.653) | copy-start | bytes 4612
  203.9 14.1 %copy-start.24 = (f32[3,128]{1,0:T(4,128)S(1)}, f32[3,128]{1,0:T(4,128)}, u32[]{:S(2)}) copy-start(f32[3,128]{1,0:T(4,128)} %slice.670) | copy-start | bytes 4612
  204.5 14.2 %copy-start.13 = (f32[7,128]{1,0:T(8,128)S(1)}, f32[7,128]{1,0:T(8,128)}, u32[]{:S(2)}) copy-start(f32[7,128]{1,0:T(8,128)} %slice.647) | copy-start | bytes 10756
  204.5 14.2 %copy-start.14 = (f32[7,128]{1,0:T(8,128)S(1)}, f32[7,128]{1,0:T(8,128)}, u32[]{:S(2)}) copy-start(f32[7,128]{1,0:T(8,128)} %slice.672) | copy-start | bytes 10756
  205.9 13.6 %copy-start.8 = (f32[15,128]{1,0:T(8,128)S(1)}, f32[15,128]{1,0:T(8,128)}, u32[]{:S(2)}) copy-start(f32[15,128]{1,0:T(8,128)} %slice.641) | copy-start | bytes 23044
  205.9 13.6 %copy-start.9 = (f32[15,128]{1,0:T(8,128)S(1)}, f32[15,128]{1,0:T(8,128)}, u32[]{:S(2)}) copy-start(f32[15,128]{1,0:T(8,128)} %slice.674) | copy-start | bytes 23044
  208.1 12.1 %copy-start.7 = (f32[31,128]{1,0:T(8,128)S(1)}, f32[31,128]{1,0:T(8,128)}, u32[]{:S(2)}) copy-start(f32[31,128]{1,0:T(8,128)} %slice.635) | copy-start | bytes 47620
  210.3 12.8 %copy-start.6 = (f32[127,128]{1,0:T(8,128)S(1)}, f32[127,128]{1,0:T(8,128)}, u32[]{:S(2)}) copy-start(f32[127,128]{1,0:T(8,128)} %slice.623) | copy-start | bytes 195076
  212.0 12.7 %copy-start.3 = (f32[255,128]{1,0:T(8,128)S(1)}, f32[255,128]{1,0:T(8,128)}, u32[]{:S(2)}) copy-start(f32[255,128]{1,0:T(8,128)} %slice.617) | copy-start | bytes 391684
  212.0 12.7 %copy-start.4 = (f32[255,128]{1,0:T(8,128)S(1)}, f32[255,128]{1,0:T(8,128)}, u32[]{:S(2)}) copy-start(f32[255,128]{1,0:T(8,128)} %slice.682) | copy-start | bytes 391684
  229.6 13.9 %copy-start.20 = (f32[2048]{0:T(1024)S(1)}, f32[2048]{0:T(1024)}, u32[]{:S(2)}) copy-start(f32[2048]{0:T(1024)} %param.17) | copy-start | bytes 24580
  247.4 9.8 %collective-permute-start.7 = (bf16[128,2048]{1,0:T(8,128)(2,1)S(1)}, bf16[128,2048]{1,0:T(8,128)(2,1)S(1)}, u32[]{:S(2)}, u32[]{:S(2)}) collective-permute-start(bf16[128,2048]{1,0:T(8,128)(2,1)S(1)} %get-tuple-element.6), channel_id=1, source_target_pairs={{0,1},{1,2},{2,3},{3,4},{4,5},{5,6},{6,7},{7,0},{8,9},{9,10},{10,1... | collective-permute-start | bytes 1572872 | tf_op jit(solution)/shard_map/ppermute | solution.py:71
  247.4 9.8 %collective-permute-start.8 = (bf16[128,2048]{1,0:T(8,128)(2,1)S(1)}, bf16[128,2048]{1,0:T(8,128)(2,1)S(1)}, u32[]{:S(2)}, u32[]{:S(2)}) collective-permute-start(bf16[128,2048]{1,0:T(8,128)(2,1)S(1)} %get-tuple-element.6), channel_id=1, source_target_pairs={{0,7},{1,0},{2,1},{3,2},{4,3},{5,4},{6,5},{7,6},{8,15},{9,8},{10,9... | collective-permute-start | bytes 1572872 | tf_op jit(solution)/shard_map/ppermute | solution.py:76
  257.2 9.8 %collective-permute-start.9 = (bf16[128,2048]{1,0:T(8,128)(2,1)S(1)}, bf16[128,2048]{1,0:T(8,128)(2,1)S(1)}, u32[]{:S(2)}, u32[]{:S(2)}) collective-permute-start(bf16[128,2048]{1,0:T(8,128)(2,1)S(1)} %collective-permute-done.7), channel_id=1, source_target_pairs={{0,1},{1,2},{2,3},{3,4},{4,5},{5,6},{6,7},{7,0},{8,9},{9,10},{10,1... | collective-permute-start | bytes 1572872 | tf_op jit(solution)/shard_map/ppermute | solution.py:71
  257.2 11.5 %collective-permute-start.10 = (bf16[128,2048]{1,0:T(8,128)(2,1)S(1)}, bf16[128,2048]{1,0:T(8,128)(2,1)S(1)}, u32[]{:S(2)}, u32[]{:S(2)}) collective-permute-start(bf16[128,2048]{1,0:T(8,128)(2,1)S(1)} %collective-permute-done.8), channel_id=1, source_target_pairs={{0,7},{1,0},{2,1},{3,2},{4,3},{5,4},{6,5},{7,6},{8,15},{9,8},{10,9... | collective-permute-start | bytes 1572872 | tf_op jit(solution)/shard_map/ppermute | solution.py:76
  267.0 9.8 %collective-permute-start.11 = (bf16[128,2048]{1,0:T(8,128)(2,1)S(1)}, bf16[128,2048]{1,0:T(8,128)(2,1)S(1)}, u32[]{:S(2)}, u32[]{:S(2)}) collective-permute-start(bf16[128,2048]{1,0:T(8,128)(2,1)S(1)} %collective-permute-done.9), channel_id=1, source_target_pairs={{0,1},{1,2},{2,3},{3,4},{4,5},{5,6},{6,7},{7,0},{8,9},{9,10},{10,1... | collective-permute-start | bytes 1572872 | tf_op jit(solution)/shard_map/ppermute | solution.py:71
  268.7 9.9 %collective-permute-start.12 = (bf16[128,2048]{1,0:T(8,128)(2,1)S(1)}, bf16[128,2048]{1,0:T(8,128)(2,1)S(1)}, u32[]{:S(2)}, u32[]{:S(2)}) collective-permute-start(bf16[128,2048]{1,0:T(8,128)(2,1)S(1)} %collective-permute-done.10), channel_id=1, source_target_pairs={{0,7},{1,0},{2,1},{3,2},{4,3},{5,4},{6,5},{7,6},{8,15},{9,8},{10,9... | collective-permute-start | bytes 1572872 | tf_op jit(solution)/shard_map/ppermute | solution.py:76
  276.9 9.8 %collective-permute-start.13 = (bf16[128,2048]{1,0:T(8,128)(2,1)S(1)}, bf16[128,2048]{1,0:T(8,128)(2,1)S(1)}, u32[]{:S(2)}, u32[]{:S(2)}) collective-permute-start(bf16[128,2048]{1,0:T(8,128)(2,1)S(1)} %collective-permute-done.11), channel_id=1, source_target_pairs={{0,1},{1,2},{2,3},{3,4},{4,5},{5,6},{6,7},{7,0},{8,9},{9,10},{10,1... | collective-permute-start | bytes 1572872 | tf_op jit(solution)/shard_map/ppermute | solution.py:71
  302.3 40.6 %copy-start.22 = (f32[2048]{0:T(1024)S(1)}, f32[2048]{0:T(1024)}, u32[]{:S(2)}) copy-start(f32[2048]{0:T(1024)} %param.19) | copy-start | bytes 24580
  (6 other events, 41.6 us)
Sparse Core Ops, SparseCore 0:
  10.4 86.7 all-gather.3
  99.3 45.7 all-gather.5
  148.1 89.4 all-gather.7
  302.4 39.1 reduce-scatter.1
